TPU v7x, 512 devices: a 4x2x32 block of a 4x8x32 slice. The times are simulated.
512 devices in a mesh: grp: 2 (over y), sp: 32 (over z), tp: 8 (over x, core).
Axes of the slice: x: 4, y: 2, z: 32, core: 2. Of those that a mesh axis runs over, the one named last changes fastest.
The devices are a block of a 4x8x32 slice.
Arguments:
- queries: bfloat16 [32768, 1024], P(('grp', 'sp'), 'tp'), parts along dimension 0, may hold values from -120 to 120
- keys: bfloat16 [32768, 256], P(('grp', 'sp')), parts along dimension 0, may hold values from -6 to 6
- values: bfloat16 [32768, 256], P(('grp', 'sp')), parts along dimension 0, may hold values from -6 to 6
- sink: float32 [8], P('tp'), may hold values from 1 to 5
- resid: bfloat16 [32768, 2048], P(('grp', 'sp')), parts along dimension 0, may hold values from -100 to 100
- out_proj: bfloat16 [1024, 2048], P(None, 'tp'), may hold values from -1.5 to 1.5
- norm_gain: float32 [2048], replicated, may hold values from 0.1 to 1.9
- w_gate: bfloat16 [2048, 6144], P('sp', 'tp'), may hold values from -0.125 to 0.125
- w_up: bfloat16 [2048, 6144], P('sp', 'tp'), may hold values from -0.125 to 0.125
- conv_w: float32 [3, 6144], P(None, 'tp'), may hold values from -3 to 3
- conv_b: float32 [6144], P('tp'), may hold values from -3 to 3
- w_down: bfloat16 [6144, 2048], P('tp', 'sp'), may hold values from -0.3125 to 0.3125
Outputs:
- layer_out: bfloat16 [32768, 2048], P(('grp', 'sp'), 'tp'), parts along dimension 0
There are 2 independent parts, one for each index of `grp`. A program takes and returns all parts, laid end to end along the dimension named above; an argument that names none is the same for every part. Nothing has to cross between parts.
All inputs are finite; a program needn't handle non-finite values.
Results may differ from a plain program's by a relative error of at most 0.015.
Values may be sent and summed in bfloat16 or wider, within the bound.
A program may use at most 64 MiB of HBM per device.

v0:
```python
import functools

import jax
import jax.numpy as jnp
from jax import lax
from jax.experimental import pallas as pl
from jax.experimental.pallas import tpu as pltpu
from jax.sharding import PartitionSpec as P

H = 8
KVH = 2
HD = 128
WINDOW = 128
CONV = 3
EDGE = 16
MESH = pl.DeviceIdType.MESH
F32 = jnp.float32
BF16 = jnp.bfloat16


def layer_kernel(
    span,
    ranks,
    q_hbm,
    k_hbm,
    v_hbm,
    sink_ref,
    res_hbm,
    op_hbm,
    gain_hbm,
    wg_hbm,
    wu_hbm,
    cw_hbm,
    cb_hbm,
    wd_hbm,
    out_ref,
    gain_ref,
    cw_ref,
    cb_ref,
    q_buf,
    kv_buf,
    res_buf,
    op_buf,
    mix_buf,
    summed,
    stat,
    nx_buf,
    wide,
    tall,
    accs,
    act_buf,
    theirs_out,
    theirs_in,
    hop_out,
    hop_in,
    held,
    out_buf,
    out_sem,
    load_sem,
    kv_send,
    kv_recv,
    z_send,
    z_recv,
    y_send,
    y_recv,
    x_send,
    x_recv,
    edge_send,
    edge_recv,
    pair_send,
    pair_recv,
    hop_send,
    hop_recv,
):
    tokens, width = res_buf.shape
    depth, hidden = wg_hbm.shape
    cols = width // ranks
    quad_of = cols // depth
    half = span // 2
    pw = wide.shape[2]
    pd = tall.shape[2]
    chips = ranks // 2

    g = lax.axis_index("grp")
    s = lax.axis_index("sp")
    t = lax.axis_index("tp")
    right, left = lax.rem(s + 1, span), lax.rem(s + span - 1, span)
    parity = lax.rem(g, 2)
    pair_grp = g + 1 - 2 * parity
    own, other = 2 * parity, 2 - 2 * parity
    core = lax.rem(t, 2)
    chip = lax.div(t, 2)
    partner = t + 1 - 2 * core
    ahead = lax.rem(t + 2 - 4 * core + ranks, ranks)
    behind = lax.rem(t - 2 + 4 * core + ranks, ranks)
    across = lax.rem(t + ranks // 2, ranks)
    kv_col = pl.multiple_of(lax.div(t * KVH, ranks) * HD, HD)

    def rows(j):
        return pl.ds(pl.multiple_of(j * depth, depth), depth)

    own_rows = rows(s)
    cut = pw - (hidden - pw)
    def own_copies(sem, pairs):
        return [pltpu.make_async_copy(src, dst, load_sem.at[sem]) for src, dst in pairs]

    def loaded(sem, ref):
        pltpu.make_async_copy(ref, ref, load_sem.at[sem]).wait()

    rest = hidden - pw
    loads = own_copies(
        0,
        [
            (wg_hbm.at[:, pl.ds(0, pw)], wide.at[0, own_rows, :]),
            (wg_hbm.at[:, pl.ds(pw, rest)], wide.at[1, own_rows, pl.ds(0, rest)]),
            (wu_hbm.at[:, pl.ds(0, cut)], wide.at[1, own_rows, pl.ds(rest, cut)]),
            (wu_hbm.at[:, pl.ds(cut, pw)], wide.at[2, own_rows, :]),
        ],
    )
    loads += own_copies(1, [(wd_hbm.at[:, pl.ds(p * pd, pd)], tall.at[p, own_rows, :]) for p in range(3)])
    loads += own_copies(
        2,
        [
            (k_hbm.at[:, pl.ds(kv_col, HD)], kv_buf.at[0, pl.ds(WINDOW, tokens), :]),
            (v_hbm.at[:, pl.ds(kv_col, HD)], kv_buf.at[1, pl.ds(WINDOW, tokens), :]),
        ],
    )
    small = [(q_hbm, q_buf), (op_hbm, op_buf.at[t]), (res_hbm, res_buf), (gain_hbm, gain_ref), (cw_hbm, cw_ref), (cb_hbm, cb_ref)]
    single = [own_copies(3 + i, [pair])[0] for i, pair in enumerate(small)]
    loads += single

    barrier = pltpu.get_barrier_semaphore()
    greeted = ({"sp": right}, {"sp": left}, {"grp": pair_grp}, {"tp": ahead}, {"tp": behind}, {"tp": partner})
    for who in greeted:
        pl.semaphore_signal(barrier, inc=1, device_id=who, device_id_type=MESH)
    for copy in loads:
        copy.start()

    def remote(src, dst, send, recv, who):
        return pltpu.make_async_remote_copy(
            src_ref=src, dst_ref=dst, send_sem=send, recv_sem=recv, device_id=who, device_id_type=MESH
        )

    def part(kind, index, j):
        return (wide if kind == 0 else tall).at[index, rows(j), :]

    def z_copy(kind, ab, j, way, turns):
        ref = part(kind, own if ab else 1, j)
        row = 2 * kind + ab
        recv = z_recv.at[way, row, lax.rem(turns, 4)]
        return remote(ref, ref, z_send.at[way, row], recv, {"sp": left if way else right})

    def y_copy(kind, j):
        ref = part(kind, own, j)
        return remote(ref, ref, y_send.at[kind], y_recv.at[kind, lax.div(j, quad_of)], {"grp": pair_grp})

    def y_arrived(kind, quad):
        def wait(n):
            buf = wide if kind == 0 else tall
            ref = buf.at[other, pl.ds(pl.multiple_of(quad * cols, cols), n * depth), :]
            remote(ref, ref, y_send.at[kind], y_recv.at[kind, quad], {"grp": pair_grp}).wait_recv()

        is_own = quad == lax.div(s, quad_of)

        @pl.when(is_own)
        def _():
            wait(quad_of - 1)

        @pl.when(jnp.logical_not(is_own))
        def _():
            wait(quad_of)

    def block(kind, b):
        if kind == 0:
            return op_buf.at[b]
        return mix_buf.at[:, pl.ds(pl.multiple_of(b * HD, HD), HD)]

    def x_copy(kind, b, slot, who):
        ref = block(kind, b)
        return remote(ref, ref, x_send.at[kind], x_recv.at[kind, b], {"tp": who})

    def x_open(kind):
        x_copy(kind, t, 0, ahead).start()
        x_copy(kind, t, 1, behind).start()
        x_copy(kind, t, 2, partner).start()

    def x_pass(kind):
        x_copy(kind, behind, 3, ahead).wait_recv()
        x_copy(kind, behind, 3, ahead).start()
        x_copy(kind, behind, 4, partner).start()
        x_copy(kind, ahead, 5, partner).wait_recv()
        x_copy(kind, ahead, 5, partner).start()

    def x_last(kind):
        x_copy(kind, across, 6, partner).wait_recv()
        x_copy(kind, across, 6, partner).start()

    def x_close(kind):
        for step in range(chips):
            b = lax.rem(partner + 2 * step, ranks)
            x_copy(kind, b, 0, partner).wait_recv()

    def kv_copy(way):
        here, there = (tokens, 0) if way == 0 else (WINDOW, WINDOW + tokens)
        src, dst = kv_buf.at[core, pl.ds(here, WINDOW), :], kv_buf.at[core, pl.ds(there, WINDOW), :]
        return remote(src, dst, kv_send, kv_recv.at[way, core], {"sp": left if way else right})

    def kv_hand(way, which):
        ref = kv_buf.at[which, pl.ds(WINDOW + tokens if way else 0, WINDOW), :]
        return remote(ref, ref, kv_send, kv_recv.at[way, which], {"tp": partner})

    side = width // 2

    def edge_copy(way):
        here, there = (tokens, 0) if way == 0 else (EDGE, EDGE + tokens)
        lanes = pl.ds(pl.multiple_of(core * side, side), side)
        src, dst = nx_buf.at[pl.ds(here, EDGE), lanes], nx_buf.at[pl.ds(there, EDGE), lanes]
        return remote(src, dst, edge_send, edge_recv.at[way, core], {"sp": left if way else right})

    def edge_hand(way, which):
        lanes = pl.ds(pl.multiple_of(which * side, side), side)
        ref = nx_buf.at[pl.ds(EDGE + tokens if way else 0, EDGE), lanes]
        return remote(ref, ref, edge_send, edge_recv.at[way, which], {"tp": partner})

    def attend(i):
        lo = i * WINDOW
        keys = kv_buf[0, lo : lo + 3 * WINDOW, :]
        vals = kv_buf[1, lo : lo + 3 * WINDOW, :]
        scores = lax.dot_general(
            q_buf[lo : lo + WINDOW, :], keys, (((1,), (1,)), ((), ())), preferred_element_type=F32
        ) * (HD ** (-0.5))
        row = lax.broadcasted_iota(jnp.int32, scores.shape, 0)
        col = lax.broadcasted_iota(jnp.int32, scores.shape, 1)
        pos = s * tokens + (lo - WINDOW) + col
        gap = col - row
        seen = (gap >= 0) & (gap <= 2 * WINDOW) & (pos >= 0) & (pos < span * tokens)
        scores = jnp.where(seen, scores, F32(-1e30))
        sink = sink_ref[0]
        top = jnp.maximum(jnp.max(scores, axis=-1, keepdims=True), sink)
        expo = jnp.exp(scores - top)
        total = jnp.sum(expo, axis=-1, keepdims=True) + jnp.exp(sink - top)
        weights = (expo / total).astype(BF16)
        mixed = jnp.dot(weights, vals, preferred_element_type=F32).astype(BF16)
        mix_buf[lo : lo + WINDOW, pl.ds(pl.multiple_of(t * HD, HD), HD)] = mixed

    def project(o, opens):
        at = pl.ds(pl.multiple_of(o * cols, cols), cols)
        block_sum = res_buf[:, at].astype(F32) + jnp.dot(mix_buf[...], op_buf[o], preferred_element_type=F32)
        summed[:, at] = block_sum
        first, second = block_sum[:, : cols // 2], block_sum[:, cols // 2 :]
        lone = first + second
        squares = first * first + second * second
        if opens:
            stat[0] = lone
            stat[1] = squares
        else:
            stat[0] += lone
            stat[1] += squares

    def normalize(lo, hi):
        @pl.loop(lo // EDGE, hi // EDGE)
        def _(i):
            at = pl.ds(pl.multiple_of(i * EDGE, EDGE), EDGE)
            mean = jnp.sum(stat[0, at, :], axis=-1, keepdims=True) / width
            msq = jnp.sum(stat[1, at, :], axis=-1, keepdims=True) / width
            scale = lax.rsqrt(msq - mean * mean + 1e-05)
            normed = (summed[at, :] - mean) * scale * gain_ref[...]
            nx_buf[pl.ds(pl.multiple_of(i * EDGE + EDGE, EDGE), EDGE), :] = normed.astype(BF16)

    mid = tokens // 2
    lots = [slice(0, mid), slice(mid, tokens)]
    parcels = [slice(q * tokens // 4, (q + 1) * tokens // 4) for q in range(4)]
    quads = span * depth // cols
    mine = lax.div(s * depth, cols)

    def gates(shift, first=False):
        quad = lax.rem(mine + shift + quads, quads)
        at = pl.ds(pl.multiple_of(quad * cols, cols), cols)

        def add(p):
            y = jnp.dot(nx_buf[:, at], wide[p, at, :], preferred_element_type=F32)
            if first:
                accs[p] = y
            else:
                accs[p] += y

        add(1)
        add(own)
        y_arrived(0, quad)
        add(other)

    def edge_zero(where):
        for p in range(2):
            accs[p, where : where + EDGE, :] = jnp.zeros((EDGE, pw), F32)

    def activate(half_of):
        for h in range(3):
            gp, gc = divmod(h * pd, pw)
            up, uc = divmod(hidden + h * pd, pw)
            for r in range(half_of * mid, (half_of + 1) * mid, WINDOW):
                conv = cb_ref[h * pd : (h + 1) * pd].reshape(1, pd)
                for tap in range(CONV):
                    lo = EDGE - CONV // 2 + tap + r
                    gate = accs[gp, lo : lo + WINDOW, gc : gc + pd].astype(BF16).astype(F32)
                    conv = conv + gate * cw_ref[tap : tap + 1, h * pd : (h + 1) * pd]
                ups = accs[up, EDGE + r : EDGE + r + WINDOW, uc : uc + pd].astype(BF16).astype(F32)
                act = conv / (1.0 + jnp.exp(-conv)) * ups
                act_buf[r : r + WINDOW, h * pd : (h + 1) * pd] = act.astype(BF16)

    def partial(o, h):
        lot = lots[h]
        if h == 0:
            y_arrived(1, o)

        at = pl.ds(pl.multiple_of(o * cols, cols), cols)
        total = None
        for p in range(3):
            term = lax.dot_general(
                act_buf[lot, p * pd : (p + 1) * pd],
                tall[p, at, :],
                (((1,), (1,)), ((), ())),
                preferred_element_type=F32,
            )
            total = term if total is None else total + term
        return total

    def pair_copy(owner, h):
        src, dst = theirs_out.at[owner, lots[h]], theirs_in.at[owner, lots[h]]
        return remote(src, dst, pair_send, pair_recv.at[owner, h], {"tp": partner})

    def hop_copy(i, q):
        src, dst = hop_out.at[i, parcels[q]], hop_in.at[i, parcels[q]]
        return remote(src, dst, hop_send, hop_recv.at[i, q], {"tp": behind if i == 1 else ahead})

    def out_copy(q):
        return pltpu.make_async_copy(out_buf.at[parcels[q], :], out_ref.at[parcels[q], :], out_sem)

    def give(owner, h):
        theirs_out[owner, lots[h]] = partial(2 * owner + 1 - core, h).astype(BF16)
        pair_copy(owner, h).start()

    def joined(owner, h):
        kept = partial(2 * owner + core, h)
        pair_copy(owner, h).wait_recv()
        return kept + theirs_in[owner, lots[h]].astype(F32)

    def hop(i, owner, h):
        hop_out[i, lots[h]] = joined(owner, h).astype(BF16)
        hop_copy(i, 2 * h).start()
        hop_copy(i, 2 * h + 1).start()

    blocks = tokens // WINDOW

    def attend_inner():
        for i in range(1, blocks - 1):
            attend(i)

    def unit_attend(inner):
        if inner:
            for way in range(2):
                kv_copy(way).wait_recv()
                kv_hand(way, core).start()
            pl.when(core == 0)(attend_inner)
        else:
            for way in range(2):
                kv_hand(way, 1 - core).wait_recv()
            attend(0)
            attend(blocks - 1)
            x_open(1)

    def unit_edge():
        for way in range(2):
            edge_copy(way).wait_recv()
            edge_hand(way, core).start()

    def mirror(b):
        return b + 1 - 2 * lax.rem(b, 2)

    def unit_project(stage):
        if stage == 0:
            x_close(1)
            for copy in single[2:]:
                copy.wait()
            project(t, True)
            project(ahead, False)
        if stage == 1:
            x_last(0)
            x_copy(0, partner, 0, partner).wait_recv()
            project(behind, False)
            project(partner, False)
        if stage == 2:
            for b in (mirror(ahead), mirror(behind)):
                x_copy(0, b, 0, partner).wait_recv()
                project(b, False)
        if stage == 3:
            x_copy(0, mirror(across), 0, partner).wait_recv()
            project(across, False)
            project(mirror(across), False)

    quarter = tokens // 4

    def unit_normalize(i, send=False):
        normalize(i * quarter, (i + 1) * quarter)
        if send:
            for way in range(2):
                edge_copy(way).start()

    def unit_gates(shifts, first=False):
        if first:
            for way in range(2):
                edge_hand(way, 1 - core).wait_recv()
        for i, shift in enumerate(shifts):
            gates(shift, first and i == 0)

    loaded(0, wide.at[:, own_rows, :])
    loaded(1, tall.at[:, own_rows, :])
    loaded(2, kv_buf.at[:, pl.ds(WINDOW, tokens), :])
    single[0].wait()
    pl.semaphore_wait(barrier, len(greeted))

    @pl.when(core == 1)
    def _():
        attend_inner()

    for kind in range(2):
        for turn in range(2):
            for way in range(2):
                z_copy(kind, turn if way == 0 else 1 - turn, s, way, 1).start()
        if kind == 0:
            for way in range(2):
                kv_copy(way).start()
    single[1].wait()
    x_open(0)

    units = {
        (1, 0): lambda: unit_attend(True),
        (1, 1): lambda: unit_attend(False),
        (3, 0): lambda: x_pass(0),
        (3, 1): lambda: x_pass(1),
        (6, 0): lambda: x_last(1),
        (6, 1): lambda: unit_project(0),
        (7, 0): lambda: unit_project(1),
        (7, 1): lambda: unit_project(2),
        (8, 0): lambda: unit_project(3),
        (8, 1): lambda: unit_normalize(0),
        (9, 0): lambda: unit_normalize(3, True),
        (9, 1): lambda: unit_normalize(1),
        (10, 0): lambda: unit_normalize(2),
        (10, 1): unit_edge,
        (11, 1): lambda: unit_gates([0], True),
        (12, 0): lambda: unit_gates([1]),
        (12, 1): lambda: unit_gates([-1]),
        (13, 0): lambda: unit_gates([2]),
        (13, 1): lambda: unit_gates([-2]),
    }

    def hop_on(kind, k, swap, turns=(0, 1)):
        back = lax.rem(s - k + span, span)
        front = lax.rem(s + k, span)
        for turn in turns:
            for way, j in ((0, back), (1, front)):
                ab = turn if way == 0 else 1 - turn
                z_copy(kind, ab, j, way, k).wait_recv()
                if ab == way:
                    z_copy(kind, ab, j, way, k + 1).start()
                else:

                    @pl.when(k < half - 1)
                    def _():
                        z_copy(kind, ab, j, way, k + 1).start()

                if ab == 1 and swap is not False:
                    pl.when(swap)(y_copy(kind, j).start)

    def swap_down(k):
        y_copy(1, lax.rem(s - k + span, span)).start()
        y_copy(1, lax.rem(s + k, span)).start()

    def ring_wide(k):
        hop_on(0, k, True)

    def ring_tall(k):
        hop_on(1, k, k < half - 1)

    @pl.loop(1, half)
    def _(k):
        ring_wide(k)
        for (step, slot), unit in units.items():
            if slot == 0:
                pl.when(k == step)(unit)

        ring_tall(k)
        for (step, slot), unit in units.items():
            if slot == 1:
                pl.when(k == step)(unit)

    far = lax.rem(s + half, span)
    z_copy(0, 1, far, 1, half).wait_recv()
    y_copy(0, far).start()
    swap_down(half - 1)
    z_copy(0, 0, far, 0, half).wait_recv()

    gates(3)
    gates(-3)
    gates(4)

    @pl.when(s == 0)
    def _():
        edge_zero(0)

    @pl.when(s == span - 1)
    def _():
        edge_zero(EDGE + tokens)

    chip_across = lax.div(across, 2)
    chip_ahead = lax.div(ahead, 2)
    chip_behind = lax.div(behind, 2)
    own_cols = pl.ds(pl.multiple_of(t * cols, cols), cols)

    activate(0)
    z_copy(1, 1, far, 1, half).wait_recv()
    y_copy(1, far).start()
    z_copy(1, 0, far, 0, half).wait_recv()
    give(chip_across, 0)
    activate(1)
    give(chip_across, 1)
    hop(0, chip_across, 0)
    give(chip_ahead, 0)
    hop(0, chip_across, 1)
    give(chip_ahead, 1)
    hop(1, chip_behind, 0)
    give(chip_behind, 0)
    hop(1, chip_behind, 1)
    give(chip_behind, 1)
    held[0, lots[0]] = joined(chip_ahead, 0)
    give(chip, 0)
    held[0, lots[1]] = joined(chip_ahead, 1)
    give(chip, 1)
    for h in range(2):
        for q in (2 * h, 2 * h + 1):
            hop_copy(0, q).wait_recv()
            hop_out[2, parcels[q]] = (held[0, parcels[q]] + hop_in[0, parcels[q]].astype(F32)).astype(BF16)
            hop_copy(2, q).start()
        own_normed = nx_buf[EDGE + h * mid : EDGE + (h + 1) * mid, own_cols].astype(F32)
        held[1, lots[h]] = joined(chip, h) + own_normed
    for q in range(4):
        hop_copy(1, q).wait_recv()
        hop_copy(2, q).wait_recv()
        terms = hop_in[1, parcels[q]].astype(F32) + hop_in[2, parcels[q]].astype(F32)
        out_buf[parcels[q], :] = (held[1, parcels[q]] + terms).astype(BF16)
        out_copy(q).start()

    pltpu.make_async_copy(out_buf, out_ref, out_sem).wait()

    def left_all(ref, send, recv):
        remote(ref, ref, send, recv, {"tp": partner}).wait_send()

    left_all(kv_buf.at[0, pl.ds(0, 4 * WINDOW), :], kv_send, kv_recv.at[0, 0])
    left_all(nx_buf.at[pl.ds(0, 2 * EDGE), :], edge_send, edge_recv.at[0, 0])
    left_all(theirs_out, pair_send, pair_recv.at[0, 0])
    left_all(hop_out, hop_send, hop_recv.at[0, 0])
    for way in range(2):
        for kind in range(2):
            for ab in range(2):
                n = half if ab == way else half - 1
                ref = (wide if kind == 0 else tall).at[0, pl.ds(0, n * depth), :]
                row = 2 * kind + ab
                remote(ref, ref, z_send.at[way, row], z_recv.at[way, row, 0], {"sp": right}).wait_send()
    for kind in range(2):
        ref = (wide if kind == 0 else tall).at[0, pl.ds(0, (span - 1) * depth), :]
        remote(ref, ref, y_send.at[kind], y_recv.at[kind, 0], {"grp": pair_grp}).wait_send()
        ref = op_buf.at[pl.ds(0, ranks - 1)] if kind == 0 else mix_buf.at[:, pl.ds(0, (ranks - 1) * HD)]
        remote(ref, ref, x_send.at[kind], x_recv.at[kind, 0], {"tp": partner}).wait_send()


def solution(mesh):
    span, ranks = mesh.shape["sp"], mesh.shape["tp"]

    def shards(q, k, v, sink, resid, out_proj, gain, w_gate, w_up, conv_w, conv_b, w_down):
        tokens, width = resid.shape
        depth, hidden = w_gate.shape
        cols = width // ranks
        chips = ranks // 2
        pw, pd = 2 * hidden // 3, hidden // 3
        there = pl.BlockSpec(memory_space=pltpu.HBM)
        scalar = pl.BlockSpec(memory_space=pltpu.SMEM)
        dma = pltpu.SemaphoreType.DMA
        return pl.pallas_call(
            functools.partial(layer_kernel, span, ranks),
            out_shape=jax.ShapeDtypeStruct((tokens, cols), BF16),
            in_specs=[there, there, there, scalar] + [there] * 8,
            out_specs=there,
            scratch_shapes=[
                pltpu.VMEM((1, width), F32),
                pltpu.VMEM(conv_w.shape, F32),
                pltpu.VMEM(conv_b.shape, F32),
                pltpu.VMEM((tokens, HD), BF16),
                pltpu.VMEM((2, tokens + 2 * WINDOW, HD), BF16),
                pltpu.VMEM((tokens, width), BF16),
                pltpu.VMEM((ranks, out_proj.shape[0], cols), BF16),
                pltpu.VMEM((tokens, ranks * HD), BF16),
                pltpu.VMEM((tokens, width), F32),
                pltpu.VMEM((2, tokens, cols // 2), F32),
                pltpu.VMEM((tokens + 2 * EDGE, width), BF16),
                pltpu.VMEM((3, span * depth, pw), BF16),
                pltpu.VMEM((3, span * depth, pd), BF16),
                pltpu.VMEM((3, tokens + 2 * EDGE, pw), F32),
                pltpu.VMEM((tokens, hidden), BF16),
                pltpu.VMEM((chips, tokens, cols), BF16),
                pltpu.VMEM((chips, tokens, cols), BF16),
                pltpu.VMEM((3, tokens, cols), BF16),
                pltpu.VMEM((3, tokens, cols), BF16),
                pltpu.VMEM((2, tokens, cols), F32),
                pltpu.VMEM((tokens, cols), BF16),
                dma(()),
                dma((9,)),
                dma(()),
                dma((2, 2)),
                dma((2, 4)),
                dma((2, 4, 4)),
                dma((2,)),
                dma((2, ranks)),
                dma((2,)),
                dma((2, ranks)),
                dma(()),
                dma((2, 2)),
                dma(()),
                dma((chips, 2)),
                dma(()),
                dma((3, 4)),
            ],
            compiler_params=pltpu.CompilerParams(
                collective_id=0, has_side_effects=True, vmem_limit_bytes=60 * 1024 * 1024
            ),
        )(
            q, k, v, sink, resid, out_proj, gain.reshape(1, width), w_gate, w_up,
            conv_w, conv_b, w_down.T,
        )

    return jax.shard_map(
        shards,
        mesh=mesh,
        in_specs=(
            P(("grp", "sp"), "tp"),
            P(("grp", "sp"), None),
            P(("grp", "sp"), None),
            P("tp"),
            P(("grp", "sp"), None),
            P(None, "tp"),
            P(),
            P("sp", "tp"),
            P("sp", "tp"),
            P(None, "tp"),
            P("tp"),
            P("tp", "sp"),
        ),
        out_specs=P(("grp", "sp"), "tp"),
        check_vma=False,
    )
```

profile of v0, /device:TPU:33, one launch (start us, length us, event | category | flops | bytes accessed | tf_op | source)
XLA Modules:
  0.0 136.7 jit_solution(10656285396125433138)
XLA Ops:
  0.7 134.3 %shard_map.118 = bf16[512,256]{1,0:T(8,128)(2,1)} custom-call(bf16[512,128]{1,0:T(8,128)(2,1)} %q_hbm.1, bf16[512,256]{1,0:T(8,128)(2,1)} %k_hbm.1, bf16[512,256]{1,0:T(8,128)(2,1)} %v_hbm.1, f32[1]{0:T(128)S(6)} %copy.14.sink_ref, bf16[512,2048]{1,0:T(8,128)(2,1)} %res_hbm.1, bf16[1024,256]{1,0:T(8,128)(2,1)} %op_hbm.1, f32[1,2048]{1,0:T(1,128)} %bitcast.3, ...), custom_call_target="tpu_custom_call" | custom-call | tf_op jit(solution)/shard_map/pallas_call | solution.py:588
  135.0 1.7 %copy.15 = bf16[512,256]{1,0:T(8,128)(2,1)} copy(bf16[512,256]{1,0:T(8,128)(2,1)} %shard_map.118) | data formatting | bytes 524288
where the time goes:
time: 137 us
  Pallas kernels  134 us (98%)
  local copies, waits for them, and re-layouts  1.67 us (1%)
    pallas_call x1, Pallas kernels, shards(): pl.pallas_call(functools.partial(layer_kernel, span, ranks), out_shape=ja...  134 us

commit v1 on v0

--- a/solution.py
+++ b/solution.py
@@ -502,6 +502,8 @@
 
     gates(3)
     gates(-3)
+    z_copy(1, 1, far, 1, half).wait_recv()
+    y_copy(1, far).start()
     gates(4)
 
     @pl.when(s == 0)
@@ -518,8 +520,6 @@
     own_cols = pl.ds(pl.multiple_of(t * cols, cols), cols)
 
     activate(0)
-    z_copy(1, 1, far, 1, half).wait_recv()
-    y_copy(1, far).start()
     z_copy(1, 0, far, 0, half).wait_recv()
     give(chip_across, 0)
     activate(1)

time: 137 us -> 137 us (level)
  no operation moved by 1% of the time
where the time goes in v1:
time: 137 us
  Pallas kernels  135 us (99%)
  local copies, waits for them, and re-layouts  1.67 us (1%)
    pallas_call x1, Pallas kernels, shards(): pl.pallas_call(functools.partial(layer_kernel, span, ranks), out_shape=ja...  135 us

profile of v1, /device:TPU:33, one launch (start us, length us, event | category | flops | bytes accessed | tf_op | source)
XLA Modules:
  0.0 136.9 jit_solution(5828973207655417090)
XLA Ops:
  0.7 134.6 %shard_map.118 = bf16[512,256]{1,0:T(8,128)(2,1)} custom-call(bf16[512,128]{1,0:T(8,128)(2,1)} %q_hbm.1, bf16[512,256]{1,0:T(8,128)(2,1)} %k_hbm.1, bf16[512,256]{1,0:T(8,128)(2,1)} %v_hbm.1, f32[1]{0:T(128)S(6)} %copy.14.sink_ref, bf16[512,2048]{1,0:T(8,128)(2,1)} %res_hbm.1, bf16[1024,256]{1,0:T(8,128)(2,1)} %op_hbm.1, f32[1,2048]{1,0:T(1,128)} %bitcast.3, ...), custom_call_target="tpu_custom_call" | custom-call | tf_op jit(solution)/shard_map/pallas_call | solution.py:588
  135.2 1.7 %copy.15 = bf16[512,256]{1,0:T(8,128)(2,1)} copy(bf16[512,256]{1,0:T(8,128)(2,1)} %shard_map.118) | data formatting | bytes 524288
